TPU v7x, 128 devices: a whole 4x4x4 slice. The times are simulated.
128 devices in a mesh: kv: 32 (over z, y, core), tp: 4 (over x).
Axes of the slice: x: 4, y: 4, z: 4, core: 2. Of those that a mesh axis runs over, the one named last changes fastest.
Arguments:
- tokens: bfloat16 [512, 4, 4096], P('kv'), may hold values from -6 to 6
- norm_gain: bfloat16 [4096], replicated, may hold values from 0.099609375 to 1.8984375
- query_weight: bfloat16 [4096, 2048], P(None, 'tp'), may hold values from -0.09375 to 0.09375
- key_weight: bfloat16 [4096, 2048], P(None, 'tp'), may hold values from -0.09375 to 0.09375
- value_weight: bfloat16 [4096, 2048], P(None, 'tp'), may hold values from -0.09375 to 0.09375
- outgate_weight: bfloat16 [4096, 2048], P(None, 'tp'), may hold values from -0.09375 to 0.09375
- gate_weight: bfloat16 [4096, 32], replicated, may hold values from -0.09375 to 0.09375
- gate_bias: float32 [2, 16], replicated, may hold values from -1 to 4
- head_gain: bfloat16 [2048], P('tp'), may hold values from 0.099609375 to 1.8984375
- out_weight: bfloat16 [2048, 4096], P('tp', 'kv'), may hold values from -0.125 to 0.125
- state_c: float32 [512, 16, 128, 128], P('kv', 'tp'), may hold values from -3 to 3
- state_n: float32 [512, 16, 128], P('kv', 'tp'), may hold values from -3 to 3
- state_m: float32 [512, 16], P('kv', 'tp'), may hold values from -1 to 2
- prev_keys: bfloat16 [512, 16, 4, 128], P('kv', 'tp'), may hold values from -6 to 6
- prev_values: bfloat16 [512, 16, 4, 128], P('kv', 'tp'), may hold values from -6 to 6
- prev_gates: float32 [512, 16, 2, 4], P('kv', 'tp'), may hold values from -2 to 5
- accepted: int32 [512], P('kv'), may hold values from 0 to 4
Outputs:
- mixed: bfloat16 [512, 4, 4096], P(None, None, 'kv')
- carried_c: float32 [512, 16, 128, 128], P('kv', 'tp')
- carried_n: float32 [512, 16, 128], P('kv', 'tp')
- carried_m: float32 [512, 16], P('kv', 'tp')
- step_keys: bfloat16 [512, 16, 4, 128], P('kv', 'tp')
- step_values: bfloat16 [512, 16, 4, 128], P('kv', 'tp')
- step_gates: float32 [512, 16, 2, 4], P('kv', 'tp')
Inputs may be any that keep to these rules, and one draw needn't show every extreme that they name: accepted counts proposals of the last step, from none to all 4.
All inputs are finite; a program needn't handle non-finite values.
Results may differ from a plain program's by a relative error of at most 0.0075.
The roundings to bfloat16 on the way count: a program that leaves them out, or rounds other values in their place, can miss the bound.
Values may be sent and summed in bfloat16 or wider, within the bound.
No kernel may reach another device: no remote copies, remote signals or barrier semaphores. Data moves between devices by JAX's collectives and lax.ppermute only.
A program may use at most 128 MiB of HBM per device.

v0:
```python
import jax
import jax.numpy as jnp
from jax import lax
from jax.sharding import PartitionSpec as P

EPSILON = 1e-06
HIGHEST = lax.Precision.HIGHEST


def joined_along(tiles, dim):
    tiles = jnp.moveaxis(tiles, 0, dim)
    lengths = tiles.shape
    return tiles.reshape(*lengths[:dim], lengths[dim] * lengths[dim + 1], *lengths[dim + 2 :])


def from_everyone(x, axis):
    peers = lax.axis_size(axis)
    return lax.all_to_all(jnp.broadcast_to(x[None], (peers, *x.shape)), axis, 0, 0, tiled=True)


def collect(x, axis, dim):
    return joined_along(from_everyone(x, axis), dim)


def replay(state_c, state_n, state_m, keys_in, values_in, gates_in, accepted):
    proposals = keys_in.shape[2]
    scaled = keys_in.astype(jnp.float32) * keys_in.shape[3] ** (-0.5)
    values_f = values_in.astype(jnp.float32)
    igates = gates_in[:, :, 0, :]
    forget = jax.nn.log_sigmoid(gates_in[:, :, 1, :])
    position = jnp.arange(proposals, dtype=jnp.int32)
    within = position[None, None, :] < accepted[:, None, None]
    masked = jnp.where(within, forget, 0.0)
    summed = jnp.sum(masked, axis=-1)
    log_weight = jnp.where(
        within, summed[..., None] - jnp.cumsum(masked, axis=-1) + igates, -jnp.inf
    )
    carried_m = jnp.maximum(summed + state_m, jnp.max(log_weight, axis=-1))
    shrink = jnp.exp(summed + state_m - carried_m)
    weights = jnp.exp(log_weight - carried_m[..., None])
    carried_c = shrink[..., None, None] * state_c + jnp.einsum(
        "bhs,bhsv,bhsd->bhvd", weights, values_f, scaled, precision=HIGHEST
    )
    carried_n = shrink[..., None] * state_n + jnp.einsum(
        "bhs,bhsd->bhd", weights, scaled, precision=HIGHEST
    )
    return (carried_c, carried_n, carried_m)


def cell_block(state_c, state_n, state_m, queries, scaled, values_f, igates, forget):
    proposals = queries.shape[2]
    cumul = jnp.cumsum(forget, axis=-1)
    causal = jnp.tril(jnp.ones((proposals, proposals), dtype=bool))
    log_decay = jnp.where(
        causal, cumul[..., :, None] - cumul[..., None, :] + igates[..., None, :], -jnp.inf
    )
    carried = cumul + state_m[..., None]
    stable = jnp.maximum(carried, jnp.max(log_decay, axis=-1))
    scores = jnp.einsum("bhtd,bhsd->bhts", queries, scaled, precision=HIGHEST) * jnp.exp(
        log_decay - stable[..., None]
    )
    weight_state = jnp.exp(carried - stable)
    numer = weight_state[..., None] * jnp.einsum(
        "bhvd,bhtd->bhtv", state_c, queries, precision=HIGHEST
    )
    numer = numer + jnp.einsum("bhts,bhsv->bhtv", scores, values_f, precision=HIGHEST)
    denom = weight_state * jnp.einsum(
        "bhd,bhtd->bht", state_n, queries, precision=HIGHEST
    ) + jnp.sum(scores, axis=-1)
    return numer / jnp.maximum(jnp.abs(denom), jnp.exp(-stable))[..., None]


def gate_heads(hidden, gain, outgate):
    heads_count = hidden.shape[1]
    head_size = hidden.shape[3]
    normed = hidden * lax.rsqrt(jnp.mean(hidden * hidden, axis=-1, keepdims=True) + EPSILON)
    normed = normed * gain.astype(jnp.float32).reshape(heads_count, head_size)[None, :, None, :]
    rows_out = jnp.transpose(normed, (0, 2, 1, 3)).reshape(outgate.shape)
    return (rows_out * jax.nn.sigmoid(outgate.astype(jnp.float32))).astype(jnp.bfloat16)


def per_device(
    tokens,
    norm_gain,
    query_weight,
    key_weight,
    value_weight,
    outgate_weight,
    gate_weight,
    gate_bias,
    head_gain,
    out_weight,
    state_c,
    state_n,
    state_m,
    prev_keys,
    prev_values,
    prev_gates,
    accepted,
):
    seqs_local, proposals, features = tokens.shape
    heads_local = state_m.shape[1]
    head_size = state_n.shape[2]
    tokens_f = tokens.astype(jnp.float32)
    normed = tokens_f * lax.rsqrt(jnp.mean(tokens_f * tokens_f, axis=-1, keepdims=True) + EPSILON)
    normed = (normed * norm_gain.astype(jnp.float32)).astype(jnp.bfloat16)
    rows_in = normed.reshape(seqs_local * proposals, features)

    def project(matrix):
        return jnp.dot(rows_in, matrix, preferred_element_type=jnp.float32).astype(jnp.bfloat16)

    def by_head(array):
        return array.reshape(seqs_local, proposals, heads_local, head_size).transpose(0, 2, 1, 3)

    queries = project(query_weight)
    keys_new = project(key_weight)
    values_new = project(value_weight)
    outgate = project(outgate_weight)
    all_gates = (
        jnp.dot(rows_in, gate_weight, preferred_element_type=jnp.float32)
        + gate_bias.reshape(-1)[None, :]
    )
    heads_total = gate_weight.shape[1] // 2
    head_offset = lax.axis_index("tp") * heads_local
    igates = lax.dynamic_slice_in_dim(all_gates, head_offset, heads_local, 1)
    fgates = lax.dynamic_slice_in_dim(all_gates, heads_total + head_offset, heads_local, 1)
    igates = igates.reshape(seqs_local, proposals, heads_local).transpose(0, 2, 1)
    fgates = fgates.reshape(seqs_local, proposals, heads_local).transpose(0, 2, 1)
    step_gates = jnp.stack([igates, fgates], axis=2)
    carried_c, carried_n, carried_m = replay(
        state_c, state_n, state_m, prev_keys, prev_values, prev_gates, accepted
    )
    step_keys = by_head(keys_new)
    step_values = by_head(values_new)
    hidden = cell_block(
        carried_c,
        carried_n,
        carried_m,
        by_head(queries).astype(jnp.float32),
        step_keys.astype(jnp.float32) * head_size ** (-0.5),
        step_values.astype(jnp.float32),
        igates,
        jax.nn.log_sigmoid(fgates),
    )
    gated = gate_heads(hidden, head_gain, outgate)
    partial_out = jnp.dot(collect(gated, "kv", 0), out_weight, preferred_element_type=jnp.float32)
    summed = lax.psum(partial_out, "tp")
    mixed = summed.astype(jnp.bfloat16).reshape(-1, proposals, summed.shape[1])
    return (mixed, carried_c, carried_n, carried_m, step_keys, step_values, step_gates)


def solution(mesh):
    in_specs = (
        P("kv", None, None),
        P(),
        P(None, "tp"),
        P(None, "tp"),
        P(None, "tp"),
        P(None, "tp"),
        P(),
        P(),
        P("tp"),
        P("tp", "kv"),
        P("kv", "tp", None, None),
        P("kv", "tp", None),
        P("kv", "tp"),
        P("kv", "tp", None, None),
        P("kv", "tp", None, None),
        P("kv", "tp", None, None),
        P("kv"),
    )
    out_specs = (
        P(None, None, "kv"),
        P("kv", "tp", None, None),
        P("kv", "tp", None),
        P("kv", "tp"),
        P("kv", "tp", None, None),
        P("kv", "tp", None, None),
        P("kv", "tp", None, None),
    )
    return jax.shard_map(
        per_device, mesh=mesh, in_specs=in_specs, out_specs=out_specs, check_vma=False
    )
```

profile of v0, /device:TPU:0, one launch (start us, length us, event | category | flops | bytes accessed | tf_op | source)
XLA Modules:
  0.0 114.7 jit_solution(9230726068473415681)
XLA Ops:
  0.6 0.0 copy-start
  0.7 0.8 add.110
  1.5 0.7 iota_compare_fusion
  2.2 0.7 bitcast_convert_fusion
  2.9 0.8 copy.77
  3.6 1.4 %fusion.7 = f32[16,4]{1,0:T(8,128)S(1)} fusion(bf16[16,4,4096]{2,1,0:T(4,128)(2,1)} %param.17), kind=kLoop, calls=%fused_computation.16 | loop fusion | flops 786368 | bytes 524544 | tf_op jit(solution)/shard_map/reduce_sum | solution.py:105
  5.0 0.7 convert_element_type.41
  5.7 0.7 fusion.41
  6.5 0.1 copy.93
  6.6 0.1 copy.76
  6.7 1.4 %fusion.9 = bf16[16,4,4096]{2,1,0:T(4,128)(2,1)S(1)} fusion(bf16[16,4,4096]{2,1,0:T(4,128)(2,1)} %param.17, f32[4096]{0:T(1024)S(1)} %convert_element_type.41, f32[16,4]{1,0:T(8,128)S(1)} %add_rsqrt_fusion), kind=kLoop, calls=%fused_computation.18 | loop fusion | flops 1048576 | bytes 1065216 | tf_op jit(solution)/shard_map/convert_element_type | solution.py:106
  8.1 0.1 reshape.103
  8.2 0.0 copy-done
  8.2 0.3 convolution_add_fusion
  8.5 0.1 reshape.104
  8.6 0.1 reshape.105
  8.7 0.1 fusion.24
  8.8 0.1 fusion.39
  8.9 2.8 %reduce_window_sum.18 = f32[16,4,4]{2,1,0:T(4,128)S(1)} reduce-window(f32[16,4,4]{2,1,0:T(4,128)S(1)} %get-tuple-element.26, f32[]{:T(128)} %constant.13.clone.1), window={size=1x1x4 pad=0_0x0_0x3_0}, to_apply=%region_3.4 | reduce-window | flops 768 | bytes 2052 | tf_op jit(solution)/shard_map/jit(cumsum)/reduce_window_sum | solution.py:36
  11.7 2.7 %reduce_window_sum.17 = f32[16,4,4]{2,1,0:T(4,128)S(1)} reduce-window(f32[16,4,4]{2,1,0:T(4,128)S(1)} %fusion.24, f32[]{:T(128)} %constant.13.clone.1), window={size=1x1x4 pad=0_0x0_0x3_0}, to_apply=%region_1.2 | reduce-window | flops 768 | bytes 2052 | tf_op jit(solution)/shard_map/jit(cumsum)/reduce_window_sum | solution.py:52
  14.4 3.0 %convolution_convert_fusion.1 = bf16[64,512]{1,0:T(8,128)(2,1)S(1)} fusion(bf16[64,4096]{1,0:T(8,128)(2,1)S(1)} %reshape.103, bf16[4096,512]{1,0:T(8,128)(2,1)} %param.21), kind=kOutput, calls=%fused_computation.12 | convolution fusion | flops 268468224 | bytes 4784128 | tf_op jit(solution)/shard_map/dot_general | solution.py:110
  17.5 0.0 copy-start.4
  17.5 3.1 %convolution_convert_fusion.2 = bf16[64,512]{1,0:T(8,128)(2,1)S(1)} fusion(bf16[64,4096]{1,0:T(8,128)(2,1)S(1)} %reshape.103, bf16[4096,512]{1,0:T(8,128)(2,1)} %param.20), kind=kOutput, calls=%fused_computation.13 | convolution fusion | flops 268468224 | bytes 4784128 | tf_op jit(solution)/shard_map/dot_general | solution.py:110
  20.6 0.0 copy-start.8
  20.6 0.0 copy-start.5
  20.6 3.1 %convolution_convert_fusion.3 = bf16[64,512]{1,0:T(8,128)(2,1)S(1)} fusion(bf16[64,4096]{1,0:T(8,128)(2,1)S(1)} %reshape.103, bf16[4096,512]{1,0:T(8,128)(2,1)} %param.19), kind=kOutput, calls=%fused_computation.14 | convolution fusion | flops 268468224 | bytes 4784128 | tf_op jit(solution)/shard_map/dot_general | solution.py:110
  23.7 0.2 fusion.38
  23.9 0.2 fusion.16
  24.1 0.1 subtract_exponential_fusion.1
  24.2 0.0 copy-done.4
  24.2 0.6 fusion.13
  24.8 0.1 copy_bitcast_fusion
  24.9 0.0 copy-start.7
  24.9 0.0 copy-start.6
  24.9 0.0 copy-done.8
  24.9 0.1 multiply_add_fusion.1
  25.0 0.0 copy-start.9
  25.0 0.4 fusion.22
  25.4 0.5 fusion.42
  25.8 0.0 copy-done.9
  25.8 0.1 exponential_maximum_fusion
  25.9 0.1 fusion.29
  26.0 0.0 copy-done.5
  26.0 9.1 %multiply_add_fusion = f32[16,4,128,128]{3,2,1,0:T(8,128)S(1)} fusion(f32[16,4,128,128]{3,2,1,0:T(8,128)} %param.27, f32[16,4]{1,0:T(8,128)S(1)} %get-tuple-element.23, bf16[16,4,4,128]{3,2,1,0:T(4,128)(2,1)S(1)} %copy-done.4, bf16[16,4,4,128]{3,2,1,0:T(4,128)(2,1)S(1)} %copy-done.5, f32[16,4,4]{2,1,0:T(4,128)S(1)} %get-tuple-element.33), kind=kOutput, calls=%fused_computation | convolution fusion | flops 52559872 | bytes 8520960 | tf_op jit(solution)/shard_map/bhs,bhsv,bhsd->bhvd/dot_general | solution.py:41
  35.1 0.0 copy-done.7
  35.2 0.0 copy-start.1
  35.2 0.0 copy-start.2
  35.2 3.3 %fusion.23 = f32[16,4,4,128]{3,2,1,0:T(4,128)S(1)} fusion(f32[16,4,128,128]{3,2,1,0:T(8,128)S(1)} %multiply_add_fusion, bf16[16,4,4,128]{3,2,1,0:T(4,128)(2,1)S(1)} %reshape.106), kind=kOutput, calls=%fused_computation.43 | convolution fusion | flops 50331648 | bytes 4390912 | tf_op jit(solution)/shard_map/bhvd,bhtd->bhtv/dot_general | solution.py:63
  38.5 0.0 copy-done.6
  38.5 0.6 fusion.17
  39.2 0.3 multiply_multiply_fusion
  39.5 0.0 copy-done.2
  39.5 0.9 fusion.6
  40.4 0.0 copy-done.1
  40.4 0.0 copy-start.3
  40.4 1.6 %broadcast_in_dim.52 = bf16[32,64,512]{2,1,0:T(8,128)(2,1)} broadcast(bf16[64,512]{1,0:T(8,128)(2,1)S(1)} %fusion.6), dimensions={1,2} | broadcast | bytes 2162688 | tf_op jit(solution)/shard_map/broadcast_in_dim | solution.py:18
  42.0 8.4 %all-to-all-start = ((bf16[32,64,512]{2,1,0:T(8,128)(2,1)}), bf16[32,64,512]{2,1,0:T(8,128)(2,1)S(1)}, u32[]{:S(2)}, u32[]{:S(2)}) async-start(bf16[32,64,512]{2,1,0:T(8,128)(2,1)} %broadcast_in_dim.52), calls=%async_computation | async-start | bytes 4194304 | tf_op jit(solution)/shard_map/all_to_all | solution.py:18
  50.4 0.7 copy.87
  51.1 0.1 copy.85
  51.2 0.1 copy.86
  51.3 0.6 pad_maximum_fusion
  51.9 28.6 %all-to-all-done = bf16[32,64,512]{2,1,0:T(8,128)(2,1)S(1)} async-done(((bf16[32,64,512]{2,1,0:T(8,128)(2,1)}), bf16[32,64,512]{2,1,0:T(8,128)(2,1)S(1)}, u32[]{:S(2)}, u32[]{:S(2)}) %all-to-all-start) | async-done | bytes 2097184 | tf_op jit(solution)/shard_map/all_to_all | solution.py:18
  80.5 0.7 fusion.43
  81.2 33.5 %all-reduce.1 = bf16[2048,128]{1,0:T(8,128)(2,1)} all-reduce(f32[2048,128]{1,0:T(8,128)S(1)} %fusion.43), channel_id=1, replica_groups=mesh['kv'=32,'tp'=4] {'tp'}, use_global_device_ids=true, to_apply=%region_8.9 | all-reduce | flops 262144 | bytes 1572864 | tf_op jit(solution)/shard_map/psum | solution.py:147
  (12 shorter events, 0.2 us)
Async XLA Ops:
  0.6 7.6 %copy-start = (bf16[4096,32]{0,1:T(8,128)(2,1)S(1)}, bf16[4096,32]{0,1:T(8,128)(2,1)}, u32[]{:S(2)}) copy-start(bf16[4096,32]{0,1:T(8,128)(2,1)} %param.23) | copy-start | bytes 786436
  17.5 6.7 %copy-start.4 = (bf16[16,4,4,128]{3,2,1,0:T(4,128)(2,1)S(1)}, bf16[16,4,4,128]{3,2,1,0:T(4,128)(2,1)}, u32[]{:S(2)}) copy-start(bf16[16,4,4,128]{3,2,1,0:T(4,128)(2,1)} %param.30) | copy-start | bytes 196612
  20.6 4.3 %copy-start.8 = (f32[16,4,128]{2,1,0:T(4,128)S(1)}, f32[16,4,128]{2,1,0:T(4,128)}, u32[]{:S(2)}) copy-start(f32[16,4,128]{2,1,0:T(4,128)} %param.28) | copy-start | bytes 98308
  20.6 5.4 %copy-start.5 = (bf16[16,4,4,128]{3,2,1,0:T(4,128)(2,1)S(1)}, bf16[16,4,4,128]{3,2,1,0:T(4,128)(2,1)}, u32[]{:S(2)}) copy-start(bf16[16,4,4,128]{3,2,1,0:T(4,128)(2,1)} %param.31) | copy-start | bytes 196612
  24.9 10.3 %copy-start.7 = (bf16[16,4,4,128]{3,2,1,0:T(4,128)(2,1)}, bf16[16,4,4,128]{3,2,1,0:T(4,128)(2,1)S(1)}, u32[]{:S(2)}) copy-start(bf16[16,4,4,128]{3,2,1,0:T(4,128)(2,1)S(1)} %get-tuple-element.40) | copy-start | bytes 196612
  24.9 13.7 %copy-start.6 = (bf16[16,4,4,128]{3,2,1,0:T(4,128)(2,1)}, bf16[16,4,4,128]{3,2,1,0:T(4,128)(2,1)S(1)}, u32[]{:S(2)}) copy-start(bf16[16,4,4,128]{3,2,1,0:T(4,128)(2,1)S(1)} %get-tuple-element.39) | copy-start | bytes 196612
  25.0 0.8 copy-start.9
  35.2 5.2 %copy-start.1 = (f32[16,4,128,128]{3,2,1,0:T(8,128)}, f32[16,4,128,128]{3,2,1,0:T(8,128)S(1)}, u32[]{:S(2)}) copy-start(f32[16,4,128,128]{3,2,1,0:T(8,128)S(1)} %multiply_add_fusion) | copy-start | bytes 12582916
  35.2 4.3 %copy-start.2 = (bf16[4096,512]{1,0:T(8,128)(2,1)S(1)}, bf16[4096,512]{1,0:T(8,128)(2,1)}, u32[]{:S(2)}) copy-start(bf16[4096,512]{1,0:T(8,128)(2,1)} %param.22) | copy-start | bytes 12582916
  40.4 40.1 %copy-start.3 = (bf16[512,128]{1,0:T(8,128)(2,1)S(1)}, bf16[512,128]{1,0:T(8,128)(2,1)}, u32[]{:S(2)}) copy-start(bf16[512,128]{1,0:T(8,128)(2,1)} %param.26) | copy-start | bytes 393220
  42.0 38.5 %all-to-all-start = ((bf16[32,64,512]{2,1,0:T(8,128)(2,1)}), bf16[32,64,512]{2,1,0:T(8,128)(2,1)S(1)}, u32[]{:S(2)}, u32[]{:S(2)}) async-start(bf16[32,64,512]{2,1,0:T(8,128)(2,1)} %broadcast_in_dim.52), calls=%async_computation | async-start | bytes 4194304 | tf_op jit(solution)/shard_map/all_to_all | solution.py:18
where the time goes:
time: 115 us
  blocking collectives  33.5 us (29%)
  waiting for transfers between devices  28.6 us (25%)
  matrix products  25.4 us (22%)
  other arithmetic  12.3 us (11%)
  starting transfers between devices  8.44 us (7%)
  local copies, waits for them, and re-layouts  5.47 us (5%)
    psum x1, blocking collectives, per_device(): summed = lax.psum(partial_out, 'tp')  33.5 us
    all_to_all x1, waiting for transfers between devices, from_everyone(): lax.all_to_all(jnp.broadcast_to(x[None], (peers, *x.shape)), axis, 0, 0,...  28.6 us
    dot_general x4, matrix products, project(): jnp.dot(rows_in, matrix, preferred_element_type=jnp.float32)  9.99 us
    dot_general x1, matrix products, replay(): jnp.einsum('bhs,bhsv,bhsd->bhvd', weights, values_f, scaled, precision=HI...  9.09 us
    all_to_all x1, starting transfers between devices, from_everyone(): lax.all_to_all(jnp.broadcast_to(x[None], (peers, *x.shape)), axis, 0, 0,...  8.44 us
    dot_general x1, matrix products, cell_block(): jnp.einsum('bhvd,bhtd->bhtv', state_c, queries, precision=HIGHEST)  3.35 us
    another operation x1, other arithmetic, replay(): jnp.cumsum(masked, axis=-1)  2.76 us
    another operation x1, other arithmetic, cell_block(): cumul = jnp.cumsum(forget, axis=-1)  2.75 us
  transfers between devices with their start and end apart: 1, of which 1 were waited for; matrix products, arithmetic and copies ran while one was open for 1% of the time, Pallas kernels for 0%

commit v1 on v0

--- a/solution.py
+++ b/solution.py
@@ -5,6 +5,11 @@
 
 EPSILON = 1e-06
 HIGHEST = lax.Precision.HIGHEST
+
+
+def gather_and_add(block, axis):
+    parts = lax.all_gather(block, axis)
+    return jnp.sum(parts, axis=0)
 
 
 def joined_along(tiles, dim):
@@ -144,7 +149,7 @@
     )
     gated = gate_heads(hidden, head_gain, outgate)
     partial_out = jnp.dot(collect(gated, "kv", 0), out_weight, preferred_element_type=jnp.float32)
-    summed = lax.psum(partial_out, "tp")
+    summed = gather_and_add(partial_out, "tp")
     mixed = summed.astype(jnp.bfloat16).reshape(-1, proposals, summed.shape[1])
     return (mixed, carried_c, carried_n, carried_m, step_keys, step_values, step_gates)
 

time: 115 us -> 143 us (1.24)
  waiting for transfers between devices: 28.6 us -> 44.6 us
  between operations: 1.02 us -> 14.4 us
  starting transfers between devices: 8.44 us -> 0.04 us
  other arithmetic: 12.3 us -> 15.7 us
  blocking collectives: 33.5 us -> 36.7 us
    all_gather x0 -> x1, waiting for transfers between devices: none -> 44.6 us  [gather_and_add(): parts = lax.all_gather(block, axis)]
    all_to_all x0 -> x1, blocking collectives: none -> 36.7 us  [from_everyone(): lax.all_to_all(jnp.broadcast_to(x[None], (peers, *x.shape)), axis, 0, 0,...]
    psum x1 -> x0, blocking collectives: 33.5 us -> none  [per_device(): summed = lax.psum(partial_out, 'tp')]
    all_to_all x1 -> x0, waiting for transfers between devices: 28.6 us -> none  [from_everyone(): lax.all_to_all(jnp.broadcast_to(x[None], (peers, *x.shape)), axis, 0, 0,...]
    all_to_all x1 -> x0, starting transfers between devices: 8.44 us -> none  [from_everyone(): lax.all_to_all(jnp.broadcast_to(x[None], (peers, *x.shape)), axis, 0, 0,...]
    reduce_sum x0 -> x1, other arithmetic: none -> 3.37 us  [gather_and_add(): return jnp.sum(parts, axis=0)]
where the time goes in v1:
time: 143 us; the launch traced here: 142 us
  waiting for transfers between devices  44.6 us (31%)
  blocking collectives  36.7 us (26%)
  matrix products  26.3 us (18%)
  other arithmetic  15.7 us (11%)
  between operations  14.4 us (10%)
  local copies, waits for them, and re-layouts  4.08 us (3%)
    all_gather x1, waiting for transfers between devices, gather_and_add(): parts = lax.all_gather(block, axis)  44.6 us
    all_to_all x1, blocking collectives, from_everyone(): lax.all_to_all(jnp.broadcast_to(x[None], (peers, *x.shape)), axis, 0, 0,...  36.7 us
    dot_general x4, matrix products, project(): jnp.dot(rows_in, matrix, preferred_element_type=jnp.float32)  9.99 us
    dot_general x1, matrix products, replay(): jnp.einsum('bhs,bhsv,bhsd->bhvd', weights, values_f, scaled, precision=HI...  9.09 us
    reduce_sum x1, other arithmetic, gather_and_add(): return jnp.sum(parts, axis=0)  3.37 us
    dot_general x1, matrix products, cell_block(): jnp.einsum('bhvd,bhtd->bhtv', state_c, queries, precision=HIGHEST)  3.35 us
  transfers between devices with their start and end apart: 1, of which 1 were waited for; matrix products, arithmetic and copies ran while one was open for 1% of the time, Pallas kernels for 0%

profile of v1, /device:TPU:0, one launch (start us, length us, event | category | flops | bytes accessed | tf_op | source)
XLA Modules:
  0.0 141.8 jit_solution(6936359981136050106)
XLA Ops:
  7.2 0.0 copy-start
  7.2 0.0 all-gather.3.cloned.1.call-start
  7.2 0.8 add.108
  8.0 0.7 iota_compare_fusion
  8.7 0.7 bitcast_convert_fusion
  9.4 0.8 copy.77
  10.2 1.4 fusion.7
  11.6 0.7 convert_element_type.45
  12.3 0.7 fusion.41
  13.0 0.1 copy.93
  13.1 0.1 copy.76
  13.2 1.4 fusion.9
  14.6 0.1 reshape.103
  14.8 0.0 copy-done
  14.8 0.3 convolution_add_fusion
  15.1 0.1 reshape.104
  15.1 0.1 reshape.105
  15.3 0.1 fusion.24
  15.3 0.1 fusion.39
  15.5 2.8 %reduce_window_sum.18 = f32[16,4,4]{2,1,0:T(4,128)S(1)} reduce-window(f32[16,4,4]{2,1,0:T(4,128)S(1)} %get-tuple-element.26, f32[]{:T(128)} %constant.13.clone.1), window={size=1x1x4 pad=0_0x0_0x3_0}, to_apply=%region_3.4 | reduce-window | flops 768 | bytes 2052 | tf_op jit(solution)/shard_map/jit(cumsum)/reduce_window_sum | solution.py:41
  18.2 2.7 %reduce_window_sum.17 = f32[16,4,4]{2,1,0:T(4,128)S(1)} reduce-window(f32[16,4,4]{2,1,0:T(4,128)S(1)} %fusion.24, f32[]{:T(128)} %constant.13.clone.1), window={size=1x1x4 pad=0_0x0_0x3_0}, to_apply=%region_1.2 | reduce-window | flops 768 | bytes 2052 | tf_op jit(solution)/shard_map/jit(cumsum)/reduce_window_sum | solution.py:57
  21.0 3.0 %convolution_convert_fusion.1 = bf16[64,512]{1,0:T(8,128)(2,1)S(1)} fusion(bf16[64,4096]{1,0:T(8,128)(2,1)S(1)} %reshape.103, bf16[4096,512]{1,0:T(8,128)(2,1)} %param.21), kind=kOutput, calls=%fused_computation.12 | convolution fusion | flops 268468224 | bytes 4784128 | tf_op jit(solution)/shard_map/dot_general | solution.py:115
  24.0 0.0 copy-start.4
  24.0 3.1 %convolution_convert_fusion.2 = bf16[64,512]{1,0:T(8,128)(2,1)S(1)} fusion(bf16[64,4096]{1,0:T(8,128)(2,1)S(1)} %reshape.103, bf16[4096,512]{1,0:T(8,128)(2,1)} %param.20), kind=kOutput, calls=%fused_computation.13 | convolution fusion | flops 268468224 | bytes 4784128 | tf_op jit(solution)/shard_map/dot_general | solution.py:115
  27.1 0.0 copy-start.8
  27.1 0.0 copy-start.5
  27.1 3.1 %convolution_convert_fusion.3 = bf16[64,512]{1,0:T(8,128)(2,1)S(1)} fusion(bf16[64,4096]{1,0:T(8,128)(2,1)S(1)} %reshape.103, bf16[4096,512]{1,0:T(8,128)(2,1)} %param.19), kind=kOutput, calls=%fused_computation.14 | convolution fusion | flops 268468224 | bytes 4784128 | tf_op jit(solution)/shard_map/dot_general | solution.py:115
  30.2 0.2 fusion.38
  30.4 0.2 fusion.16
  30.7 0.1 subtract_exponential_fusion.1
  30.8 0.0 copy-done.4
  30.8 0.6 fusion.13
  31.3 0.1 copy_bitcast_fusion
  31.4 0.0 copy-start.7
  31.4 0.0 copy-start.6
  31.4 0.0 copy-done.8
  31.4 0.1 multiply_add_fusion.1
  31.5 0.0 copy-start.9
  31.5 0.3 fusion.22
  31.9 0.5 fusion.42
  32.3 0.1 exponential_maximum_fusion
  32.5 0.1 fusion.29
  32.6 0.0 copy-done.5
  32.6 9.1 %multiply_add_fusion = f32[16,4,128,128]{3,2,1,0:T(8,128)S(1)} fusion(f32[16,4,128,128]{3,2,1,0:T(8,128)} %param.27, f32[16,4]{1,0:T(8,128)S(1)} %get-tuple-element.23, bf16[16,4,4,128]{3,2,1,0:T(4,128)(2,1)S(1)} %copy-done.4, bf16[16,4,4,128]{3,2,1,0:T(4,128)(2,1)S(1)} %copy-done.5, f32[16,4,4]{2,1,0:T(4,128)S(1)} %get-tuple-element.33), kind=kOutput, calls=%fused_computation | convolution fusion | flops 52559872 | bytes 8520960 | tf_op jit(solution)/shard_map/bhs,bhsv,bhsd->bhvd/dot_general | solution.py:46
  41.7 0.0 copy-done.7
  41.7 0.0 copy-done.9
  41.7 0.0 copy-start.1
  41.7 0.0 copy-start.2
  41.7 3.3 %fusion.23 = f32[16,4,4,128]{3,2,1,0:T(4,128)S(1)} fusion(f32[16,4,128,128]{3,2,1,0:T(8,128)S(1)} %multiply_add_fusion, bf16[16,4,4,128]{3,2,1,0:T(4,128)(2,1)S(1)} %reshape.106), kind=kOutput, calls=%fused_computation.43 | convolution fusion | flops 50331648 | bytes 4390912 | tf_op jit(solution)/shard_map/bhvd,bhtd->bhtv/dot_general | solution.py:68
  45.1 0.6 fusion.17
  45.7 0.3 multiply_multiply_fusion
  46.0 0.9 fusion.6
  46.9 0.0 copy-done.1
  46.9 0.0 copy-start.3
  46.9 0.2 broadcast_in_dim.52
  47.2 36.7 %all_to_all.5 = bf16[32,64,512]{2,1,0:T(8,128)(2,1)S(1)} all-to-all(bf16[32,64,512]{2,1,0:T(8,128)(2,1)S(1)} %broadcast_in_dim.52), channel_id=1, replica_groups=mesh['kv'=32,'tp'=4] {'kv'}, dimensions={0} | all-to-all | bytes 4194304 | tf_op jit(solution)/shard_map/all_to_all | solution.py:23
  83.9 1.7 %fusion.43 = f32[2048,128]{1,0:T(8,128)} fusion(bf16[2048,512]{1,0:T(8,128)(2,1)S(1)} %bitcast.129, bf16[512,128]{1,0:T(8,128)(2,1)S(1)} %copy-done.3), kind=kOutput, calls=%fused_computation.84 | convolution fusion | flops 268435456 | bytes 3276800 | tf_op jit(solution)/shard_map/dot_general | solution.py:151
  85.5 0.0 all-gather.3.cloned.1.call-update
  85.6 0.7 copy.87
  86.2 0.1 copy.85
  86.3 0.1 copy.86
  86.4 0.6 pad_maximum_fusion
  87.1 44.6 %all-gather.3.cloned.1.call-done = f32[8192,128]{1,0:T(8,128)} async-done(((f32[2048,128]{1,0:T(8,128)}), f32[8192,128]{1,0:T(8,128)}) %all-gather.3.cloned.1.call-update) | async-done | bytes 4194320 | tf_op jit(solution)/shard_map/all_gather | solution.py:11
  131.6 3.4 %reduce_sum.52 = bf16[2048,128]{1,0:T(8,128)(2,1)} reduce(f32[4,2048,128]{2,1,0:T(8,128)} %bitcast.130, f32[]{:T(128)} %constant.13.clone.1), dimensions={0}, to_apply=%region_8.9 | reduce | flops 786432 | bytes 4718596 | tf_op jit(solution)/shard_map/reduce_sum | solution.py:12
  (14 shorter events, 0.2 us)
Async XLA Ops:
  7.2 7.6 %copy-start = (bf16[4096,32]{0,1:T(8,128)(2,1)S(1)}, bf16[4096,32]{0,1:T(8,128)(2,1)}, u32[]{:S(2)}) copy-start(bf16[4096,32]{0,1:T(8,128)(2,1)} %param.23) | copy-start | bytes 786436
  7.2 124.5 %all-gather.3.cloned.1.call-start = ((), (), s32[]{:S(2)}) async-start(), calls=%async_computation.1 | async-start | bytes 5242880 | tf_op jit(solution)/shard_map/all_gather | solution.py:11
  24.0 6.7 %copy-start.4 = (bf16[16,4,4,128]{3,2,1,0:T(4,128)(2,1)S(1)}, bf16[16,4,4,128]{3,2,1,0:T(4,128)(2,1)}, u32[]{:S(2)}) copy-start(bf16[16,4,4,128]{3,2,1,0:T(4,128)(2,1)} %param.30) | copy-start | bytes 196612
  27.1 4.3 %copy-start.8 = (f32[16,4,128]{2,1,0:T(4,128)S(1)}, f32[16,4,128]{2,1,0:T(4,128)}, u32[]{:S(2)}) copy-start(f32[16,4,128]{2,1,0:T(4,128)} %param.28) | copy-start | bytes 98308
  27.1 5.4 %copy-start.5 = (bf16[16,4,4,128]{3,2,1,0:T(4,128)(2,1)S(1)}, bf16[16,4,4,128]{3,2,1,0:T(4,128)(2,1)}, u32[]{:S(2)}) copy-start(bf16[16,4,4,128]{3,2,1,0:T(4,128)(2,1)} %param.31) | copy-start | bytes 196612
  31.4 10.3 %copy-start.7 = (bf16[16,4,4,128]{3,2,1,0:T(4,128)(2,1)}, bf16[16,4,4,128]{3,2,1,0:T(4,128)(2,1)S(1)}, u32[]{:S(2)}) copy-start(bf16[16,4,4,128]{3,2,1,0:T(4,128)(2,1)S(1)} %get-tuple-element.40) | copy-start | bytes 196612
  31.4 13.7 %copy-start.6 = (bf16[16,4,4,128]{3,2,1,0:T(4,128)(2,1)}, bf16[16,4,4,128]{3,2,1,0:T(4,128)(2,1)S(1)}, u32[]{:S(2)}) copy-start(bf16[16,4,4,128]{3,2,1,0:T(4,128)(2,1)S(1)} %get-tuple-element.39) | copy-start | bytes 196612
  31.5 10.2 %copy-start.9 = (f32[16,4,128]{2,1,0:T(4,128)}, f32[16,4,128]{2,1,0:T(4,128)S(1)}, u32[]{:S(2)}) copy-start(f32[16,4,128]{2,1,0:T(4,128)S(1)} %multiply_add_fusion.1) | copy-start | bytes 98308
  41.7 5.2 %copy-start.1 = (f32[16,4,128,128]{3,2,1,0:T(8,128)}, f32[16,4,128,128]{3,2,1,0:T(8,128)S(1)}, u32[]{:S(2)}) copy-start(f32[16,4,128,128]{3,2,1,0:T(8,128)S(1)} %multiply_add_fusion) | copy-start | bytes 12582916
  41.7 4.3 %copy-start.2 = (bf16[4096,512]{1,0:T(8,128)(2,1)S(1)}, bf16[4096,512]{1,0:T(8,128)(2,1)}, u32[]{:S(2)}) copy-start(bf16[4096,512]{1,0:T(8,128)(2,1)} %param.22) | copy-start | bytes 12582916
  46.9 36.9 %copy-start.3 = (bf16[512,128]{1,0:T(8,128)(2,1)S(1)}, bf16[512,128]{1,0:T(8,128)(2,1)}, u32[]{:S(2)}) copy-start(bf16[512,128]{1,0:T(8,128)(2,1)} %param.26) | copy-start | bytes 393220
Sparse Core Ops, SparseCore 0:
  85.7 45.8 all-gather.2
